TPU v7x, 256 devices: a whole 4x4x8 slice. The times are simulated.
256 devices in a mesh: sp: 64 (over z, y, core), tp: 4 (over x).
Axes of the slice: x: 4, y: 4, z: 8, core: 2. Of those that a mesh axis runs over, the one named last changes fastest.
Arguments:
- out_cotangent: bfloat16 [8192, 2048], P('sp'), may hold values from -16 to 16
- routes: int32 [8192, 2], P('sp'), may hold values from 0 to 63, all different within a row; in each aligned block of 128 rows (0 to 127, 128 to 255, ...) at most 6 rows name the same one
- route_weights: float32 [8192, 2], P('sp'), may hold values from 0.3 to 1.5
- expert_rows: bfloat16 [64, 384, 2048], P('sp', None, 'tp'), may hold values from -6 to 6
- w_gate: bfloat16 [64, 2048, 1024], P('sp', None, 'tp'), may hold values from -0.125 to 0.125
- w_up: bfloat16 [64, 2048, 1024], P('sp', None, 'tp'), may hold values from -0.125 to 0.125
- w_down: bfloat16 [64, 1024, 2048], P('sp', 'tp'), may hold values from -0.1875 to 0.1875
- out_weight: bfloat16 [2048, 4096], P('sp', 'tp'), may hold values from -0.09375 to 0.09375
- values: bfloat16 [8192, 4096], P('sp', 'tp'), may hold values from -0.25 to 0.25
- keys: bfloat16 [8192, 1024], P('sp', 'tp'), may hold values from -0.5 to 0.5
- queries: bfloat16 [8192, 1024], P('sp', 'tp'), may hold values from -6 to 6
- log_decay: float32 [8192, 64], P('sp', 'tp'), may hold values from -1 to 0
- gate_input: bfloat16 [8192, 4096], P('sp', 'tp'), may hold values from -6 to 6
Outputs:
- grad_w_gate: bfloat16 [64, 2048, 1024], P('sp', None, 'tp')
- grad_w_up: bfloat16 [64, 2048, 1024], P('sp', None, 'tp')
- grad_w_down: bfloat16 [64, 1024, 2048], P('sp', 'tp')
- grad_out_weight: float32 [2048, 4096], P('sp', 'tp')
- grad_residual: float32 [8192, 2048], P('sp', 'tp')
- grad_values: float32 [8192, 4096], P('sp', 'tp')
- grad_keys: float32 [8192, 1024], P('sp', 'tp')
- grad_queries: float32 [8192, 1024], P('sp', 'tp')
- grad_decay: float32 [8192, 64], P('sp', 'tp')
- grad_gate: float32 [8192, 4096], P('sp', 'tp')
Inputs may be any that keep to these rules, and one draw needn't show every extreme that they name: `routes`: in each aligned block of 128 tokens no expert is named by more than 6 pairs, a bound that some block reaches.
All inputs are finite; a program needn't handle non-finite values.
Results may differ from a plain program's by a relative error of at most 0.0062.
Values may be sent and summed in bfloat16 or wider, within the bound.
A program may use at most 128 MiB of HBM per device.

v0:
```python
import jax
import jax.numpy as jnp
from jax import lax
from jax.sharding import Mesh
from jax.sharding import PartitionSpec as P

STATE = 128
SPAN = 128
SP = ("sp_0", "sp_1", "sp_2")
HIGHEST = lax.Precision.HIGHEST


def nothing_yet(shard, identity):
    return jax.tree.map(
        lambda part, zero: jnp.zeros_like(part) + jnp.asarray(zero, part.dtype), shard, identity
    )


def carried_in(shard, axes, combine, identity, reverse):
    before = start = nothing_yet(shard, identity)
    running = shard
    for axis in reversed(axes):
        length, here = (lax.axis_size(axis), lax.axis_index(axis))
        pieces = jax.tree.map(lambda part: lax.all_gather(part, axis), running)
        inside, running = (start, start)
        for k in reversed(range(length)) if reverse else range(length):
            passed = k > here if reverse else k < here
            running = combine(running, jax.tree.map(lambda part: part[k], pieces))
            inside = jax.tree.map(lambda new, old: jnp.where(passed, new, old), running, inside)
        before = combine(inside, before)
    return before


def block_step(state_now, block_input):
    values_blk, keys_blk, queries_blk, decay_blk = block_input
    span_len, head_count, head_dim = values_blk.shape
    groups = keys_blk.shape[1]
    state_dim = keys_blk.shape[2]
    repeat = head_count // groups
    cumulative = jnp.cumsum(decay_blk, axis=0)
    lower_mask = jnp.arange(span_len)[:, None] >= jnp.arange(span_len)[None, :]
    segment = cumulative[:, None, :] - cumulative[None, :, :]
    weights = jnp.exp(jnp.where(lower_mask[:, :, None], segment, -jnp.inf)).reshape(
        span_len, span_len, groups, repeat
    )
    inner_prod = jnp.einsum("tgn,sgn->tsg", queries_blk, keys_blk, precision=HIGHEST)
    grouped = values_blk.reshape(span_len, groups, repeat, head_dim)
    combined = inner_prod[:, :, :, None] * weights
    within = jnp.einsum("tsgr,sgrp->tgrp", combined, grouped, precision=HIGHEST)
    carried = jnp.einsum(
        "tgn,grpn->tgrp",
        queries_blk,
        state_now.reshape(groups, repeat, head_dim, state_dim),
        precision=HIGHEST,
    )
    carried = carried * jnp.exp(cumulative).reshape(span_len, groups, repeat)[..., None]
    to_end = jnp.exp(cumulative[-1][None, :] - cumulative).reshape(span_len, groups, repeat)
    added_state = jnp.einsum(
        "sgn,sgrp->grpn", keys_blk, grouped * to_end[..., None], precision=HIGHEST
    )
    new_state = state_now * jnp.exp(cumulative[-1])[:, None, None] + added_state.reshape(
        head_count, head_dim, state_dim
    )
    return (new_state, (within + carried).reshape(span_len, head_count * head_dim))


def mixer_scan(value_f, key_f, query_f, decay_f, start_state):
    row_count = value_f.shape[0]
    head_count = decay_f.shape[1]
    groups = key_f.shape[1] // STATE
    head_dim = value_f.shape[1] // head_count
    span_len = min(SPAN, row_count)
    blocks = row_count // span_len
    value_b = value_f.reshape(blocks, span_len, head_count, head_dim)
    key_b = key_f.reshape(blocks, span_len, groups, STATE)
    query_b = query_f.reshape(blocks, span_len, groups, STATE)
    decay_b = decay_f.reshape(blocks, span_len, head_count)
    end_state, outputs = lax.scan(block_step, start_state, (value_b, key_b, query_b, decay_b))
    return (outputs.reshape(row_count, head_count * head_dim), end_state)


def carry_combine(earlier, later):
    return (earlier[0] * later[0], later[0][:, None, None] * earlier[1] + later[1])


def shards(
    out_cotangent,
    routes,
    route_weights,
    expert_rows,
    w_gate,
    w_up,
    w_down,
    out_weight,
    values,
    keys,
    queries,
    log_decay,
    gate_input,
):
    sp_size = lax.axis_size(SP)
    tp_size = lax.axis_size("tp")
    tok_count, model_width = out_cotangent.shape
    local_experts = w_gate.shape[0]
    slot_count = expert_rows.shape[1]
    capacity = slot_count // sp_size
    experts_all = local_experts * sp_size
    columns = model_width // tp_size
    pair_list = routes.reshape(-1)
    onehot = (pair_list[:, None] == jnp.arange(experts_all, dtype=jnp.int32)[None, :]).astype(
        jnp.int32
    )
    pair_rank = jnp.sum(jnp.cumsum(onehot, axis=0) * onehot, axis=1) - 1
    target = pair_list * capacity + pair_rank
    cotangent_part = lax.dynamic_slice_in_dim(
        out_cotangent, lax.axis_index("tp") * columns, columns, 1
    )
    scaled = (route_weights[:, :, None] * cotangent_part[:, None, :].astype(jnp.float32)).astype(
        jnp.bfloat16
    )
    outgoing = (
        jnp.zeros((experts_all * capacity, columns), jnp.bfloat16)
        .at[target]
        .set(scaled.reshape(-1, columns))
    )
    arrived_part = lax.all_to_all(
        outgoing.reshape(experts_all, capacity, columns),
        SP,
        split_axis=0,
        concat_axis=0,
        tiled=True,
    )
    arrived_part = jnp.moveaxis(
        arrived_part.reshape(sp_size, local_experts, capacity, columns), 0, 1
    )
    arrived_part = arrived_part.reshape(local_experts, slot_count, columns)
    arrived = lax.all_gather(arrived_part, "tp", axis=2, tiled=True)
    full_rows = lax.all_gather(expert_rows, "tp", axis=2, tiled=True)
    gate_pre = jnp.einsum("esd,edf->esf", full_rows, w_gate, preferred_element_type=jnp.float32)
    up_pre = jnp.einsum("esd,edf->esf", full_rows, w_up, preferred_element_type=jnp.float32)
    sigmoid_gate = jax.nn.sigmoid(gate_pre)
    activated = gate_pre * sigmoid_gate
    hidden = (activated * up_pre).astype(jnp.bfloat16)
    hidden_grad = jnp.einsum("esd,efd->esf", arrived, w_down, preferred_element_type=jnp.float32)
    slope = sigmoid_gate * (1.0 + gate_pre * (1.0 - sigmoid_gate))
    gate_grad = (hidden_grad * up_pre * slope).astype(jnp.bfloat16)
    up_grad = (hidden_grad * activated).astype(jnp.bfloat16)
    grad_w_down = jnp.einsum(
        "esf,esd->efd", hidden, arrived, preferred_element_type=jnp.float32
    ).astype(jnp.bfloat16)
    grad_w_gate = jnp.einsum(
        "esd,esf->edf", full_rows, gate_grad, preferred_element_type=jnp.float32
    ).astype(jnp.bfloat16)
    grad_w_up = jnp.einsum(
        "esd,esf->edf", full_rows, up_grad, preferred_element_type=jnp.float32
    ).astype(jnp.bfloat16)
    partial_value = jnp.einsum(
        "esf,edf->esd", gate_grad, w_gate, preferred_element_type=jnp.float32
    )
    partial_value = partial_value + jnp.einsum(
        "esf,edf->esd", up_grad, w_up, preferred_element_type=jnp.float32
    )
    summed = lax.psum_scatter(partial_value, "tp", scatter_dimension=2, tiled=True).astype(
        jnp.bfloat16
    )
    send_back = jnp.moveaxis(summed.reshape(local_experts, sp_size, capacity, columns), 1, 0)
    send_back = send_back.reshape(experts_all, capacity, columns)
    returned = lax.all_to_all(send_back, SP, split_axis=0, concat_axis=0, tiled=True)
    picked = returned.reshape(experts_all * capacity, columns)[target].reshape(
        tok_count, -1, columns
    )
    own_columns = lax.dynamic_slice_in_dim(
        out_cotangent, lax.axis_index("tp") * columns, columns, 1
    )
    grad_residual = own_columns.astype(jnp.float32) + jnp.sum(picked.astype(jnp.float32), axis=1)
    residual_low = lax.all_gather(grad_residual.astype(jnp.bfloat16), "tp", axis=1, tiled=True)
    head_count = log_decay.shape[1]
    groups = keys.shape[1] // STATE
    head_dim = values.shape[1] // head_count
    repeat = head_count // groups
    value_f = values.astype(jnp.float32)
    key_f = keys.astype(jnp.float32)
    query_f = queries.astype(jnp.float32)
    cumulative = jnp.cumsum(log_decay, axis=0)
    decay_total = jnp.exp(cumulative[-1])
    to_end = jnp.exp(cumulative[-1][None, :] - cumulative)
    scaled_values = (value_f.reshape(tok_count, head_count, head_dim) * to_end[:, :, None]).reshape(
        tok_count, groups, repeat, head_dim
    )
    own_state = jnp.einsum(
        "sgn,sgrp->grpn", key_f.reshape(tok_count, groups, STATE), scaled_values, precision=HIGHEST
    )
    own_state = own_state.reshape(head_count, head_dim, STATE)
    identity = (
        jnp.ones((head_count,), jnp.float32),
        jnp.zeros((head_count, head_dim, STATE), jnp.float32),
    )
    entry_state = carried_in((decay_total, own_state), SP, carry_combine, identity, False)[1]
    (mixer_y, leaving), pull_back = jax.vjp(
        mixer_scan, value_f, key_f, query_f, log_decay, entry_state
    )
    part_rows = residual_low
    mixed_grad = jnp.dot(
        part_rows,
        lax.all_gather(out_weight, SP, axis=0, tiled=True),
        preferred_element_type=jnp.float32,
    )
    gate_f = gate_input.astype(jnp.float32)
    gate_sigmoid = jax.nn.sigmoid(gate_f)
    gate_active = gate_f * gate_sigmoid
    gate_slope = gate_sigmoid * (1.0 + gate_f * (1.0 - gate_sigmoid))
    mixed = (mixer_y * gate_active).astype(jnp.bfloat16)
    grad_gate = mixed_grad * mixer_y * gate_slope
    y_grad = mixed_grad * gate_active
    weighted_grad = (
        y_grad.reshape(tok_count, head_count, head_dim) * jnp.exp(cumulative)[:, :, None]
    ).reshape(tok_count, groups, repeat, head_dim)
    reached_state = jnp.einsum(
        "tgn,tgrp->grpn",
        query_f.reshape(tok_count, groups, STATE),
        weighted_grad,
        precision=HIGHEST,
    )
    reached_state = reached_state.reshape(head_count, head_dim, STATE)
    later_state = carried_in((decay_total, reached_state), SP, carry_combine, identity, True)[1]
    grad_values, grad_keys, grad_queries, grad_decay, unused_state = pull_back(
        (y_grad, later_state)
    )
    part_rows = residual_low
    grad_out_weight = lax.psum_scatter(
        lax.dot_general(
            part_rows, mixed, (((0,), (0,)), ((), ())), preferred_element_type=jnp.float32
        ),
        SP,
        scatter_dimension=0,
        tiled=True,
    )
    return (
        grad_w_gate,
        grad_w_up,
        grad_w_down,
        grad_out_weight,
        grad_residual,
        grad_values,
        grad_keys,
        grad_queries,
        grad_decay,
        grad_gate,
    )


def solution(mesh):
    finer = Mesh(mesh.devices.reshape(8, 4, 2, mesh.shape["tp"]), ("sp_0", "sp_1", "sp_2", "tp"))
    in_specs = (
        P(SP, None),
        P(SP, None),
        P(SP, None),
        P(SP, None, "tp"),
        P(SP, None, "tp"),
        P(SP, None, "tp"),
        P(SP, "tp", None),
        P(SP, "tp"),
        P(SP, "tp"),
        P(SP, "tp"),
        P(SP, "tp"),
        P(SP, "tp"),
        P(SP, "tp"),
    )
    out_specs = (
        P(SP, None, "tp"),
        P(SP, None, "tp"),
        P(SP, "tp", None),
        P(SP, "tp"),
        P(SP, "tp"),
        P(SP, "tp"),
        P(SP, "tp"),
        P(SP, "tp"),
        P(SP, "tp"),
        P(SP, "tp"),
    )
    return jax.shard_map(
        shards, mesh=finer, in_specs=in_specs, out_specs=out_specs, check_vma=False
    )
```

profile of v0, /device:TPU:4, one launch (start us, length us, event | category | flops | bytes accessed | tf_op | source)
XLA Modules:
  0.0 573.2 jit_solution(100809377200915807)
XLA Ops:
  16.1 29.5 %all_to_all.10 = bf16[64,6,512]{2,1,0:T(8,128)(2,1)S(1)} all-to-all(bf16[64,6,512]{2,1,0:T(8,128)(2,1)S(1)} %reshape.691), channel_id=1, replica_groups=mesh['sp_0'=8,'sp_1'=4,'sp_2'=2,'tp'=4] {'sp_0','sp_1','sp_2'}, dimensions={0} | all-to-all | bytes 786432 | tf_op jit(solution)/shard_map/all_to_all | solution.py:126
  50.7 22.0 %all-gather.14.cloned.1.call-done = bf16[1,384,2048]{2,1,0:T(8,128)(2,1)} async-done(((bf16[1,384,512]{2,1,0:T(8,128)(2,1)}), bf16[1,384,2048]{2,1,0:T(8,128)(2,1)}) %all-gather.14.cloned.1.call-update) | async-done | bytes 1572880 | tf_op jit(solution)/shard_map/all_gather | solution.py:137
  72.7 2.3 multiply_convert_fusion.3
  76.4 2.2 add_bitcast_fusion
  79.3 40.2 %reduce-scatter.3.cloned.1.call-done = f32[1,384,512]{2,1,0:T(8,128)} async-done(((f32[1,384,2048]{2,1,0:T(8,128)}), f32[1,384,512]{2,1,0:T(8,128)}) %reduce-scatter.3.cloned.1.call-update) | async-done | bytes 786448 | tf_op jit(solution)/shard_map/reduce_scatter | solution.py:163
  121.5 10.5 %all-to-all-start.1 = ((bf16[64,6,512]{2,1,0:T(8,128)(2,1)}), bf16[64,6,512]{2,1,0:T(8,128)(2,1)S(1)}, u32[]{:S(2)}, u32[]{:S(2)}) async-start(bf16[64,6,512]{2,1,0:T(8,128)(2,1)} %reshape_transpose_reshape.7), calls=%async_computation.2 | async-start | bytes 1048576 | tf_op jit(solution)/shard_map/all_to_all | solution.py:168
  132.5 21.9 %all-to-all-done.1 = bf16[64,6,512]{2,1,0:T(8,128)(2,1)S(1)} async-done(((bf16[64,6,512]{2,1,0:T(8,128)(2,1)}), bf16[64,6,512]{2,1,0:T(8,128)(2,1)S(1)}, u32[]{:S(2)}, u32[]{:S(2)}) %all-to-all-start.1) | async-done | bytes 393248 | tf_op jit(solution)/shard_map/all_to_all | solution.py:168
  158.3 11.8 %all_gather.56 = bf16[128,2048]{1,0:T(8,128)(2,1)S(1)} all-gather(bf16[128,512]{1,0:T(8,128)(2,1)S(1)} %get-tuple-element.222), channel_id=1, replica_groups=mesh['sp_0'=8,'sp_1'=4,'sp_2'=2,'tp'=4] {'tp'}, dimensions={1}, use_global_device_ids=true | all-gather | bytes 655360 | tf_op jit(solution)/shard_map/all_gather | solution.py:176
  170.1 4.0 fusion.72
  178.5 10.4 %all-gather.1 = f32[4,1,16]{2,1,0:T(1,128)S(1)} all-gather(f32[1,1,16]{2,1,0:T(1,128)S(1)} %get-tuple-element.301), channel_id=1, replica_groups=mesh['sp_0'=8,'sp_1'=4,'sp_2'=2,'tp'=4] {'sp_1'}, dimensions={0}, use_global_device_ids=true | all-gather | bytes 320 | tf_op jit(solution)/shard_map/all_gather | solution.py:24
  189.5 2.3 multiply_add_fusion.1
  192.5 31.9 %all-gather.28.cloned.1.call-done = f32[4,16,64,128]{3,2,1,0:T(8,128)} async-done(((f32[1,16,64,128]{3,2,1,0:T(8,128)}), f32[4,16,64,128]{3,2,1,0:T(8,128)}) %all-gather.28.cloned.1.call-update) | async-done | bytes 2097168 | tf_op jit(solution)/shard_map/all_gather | solution.py:24
  224.4 3.3 multiply_add_fusion
  229.6 16.8 %all-gather.3 = f32[8,1,16]{2,1,0:T(1,128)S(1)} all-gather(f32[1,1,16]{2,1,0:T(1,128)S(1)} %get-tuple-element.282), channel_id=1, replica_groups=mesh['sp_0'=8,'sp_1'=4,'sp_2'=2,'tp'=4] {'sp_0'}, dimensions={0}, use_global_device_ids=true | all-gather | bytes 576 | tf_op jit(solution)/shard_map/all_gather | solution.py:24
  253.0 29.7 %all-gather.30.cloned.1.call-done = f32[8,16,64,128]{3,2,1,0:T(8,128)} async-done(((f32[1,16,64,128]{3,2,1,0:T(8,128)}), f32[8,16,64,128]{3,2,1,0:T(8,128)}) %all-gather.30.cloned.1.call-update) | async-done | bytes 4194320 | tf_op jit(solution)/shard_map/all_gather | solution.py:24
  282.9 2.6 fusion.102
  285.8 2.6 add_add_fusion
  291.5 12.9 %all-gather.18.cloned.1.call-done = f32[2,16,64,128]{3,2,1,0:T(8,128)} async-done(((f32[1,16,64,128]{3,2,1,0:T(8,128)}), f32[2,16,64,128]{3,2,1,0:T(8,128)}) %all-gather.18.cloned.1.call-update) | async-done | bytes 1048592 | tf_op jit(solution)/shard_map/all_gather | solution.py:24
  304.5 2.4 multiply_add_fusion.3
  307.0 34.6 %all-gather.20.cloned.1.call-done = f32[4,16,64,128]{3,2,1,0:T(8,128)} async-done(((f32[1,16,64,128]{3,2,1,0:T(8,128)}), f32[4,16,64,128]{3,2,1,0:T(8,128)}) %all-gather.20.cloned.1.call-update) | async-done | bytes 2097168 | tf_op jit(solution)/shard_map/all_gather | solution.py:24
  341.6 3.2 multiply_add_fusion.2
  345.2 16.7 %all-gather.2 = f32[8,1,16]{2,1,0:T(1,128)S(1)} all-gather(f32[1,1,16]{2,1,0:T(1,128)S(1)} %copy-done.91), channel_id=1, replica_groups=mesh['sp_0'=8,'sp_1'=4,'sp_2'=2,'tp'=4] {'sp_0'}, dimensions={0}, use_global_device_ids=true | all-gather | bytes 576 | tf_op jit(solution)/shard_map/all_gather | solution.py:24
  369.3 30.4 %all-gather.22.cloned.1.call-done = f32[8,16,64,128]{3,2,1,0:T(8,128)} async-done(((f32[1,16,64,128]{3,2,1,0:T(8,128)}), f32[8,16,64,128]{3,2,1,0:T(8,128)}) %all-gather.22.cloned.1.call-update) | async-done | bytes 4194320 | tf_op jit(solution)/shard_map/all_gather | solution.py:24
  400.0 2.6 fusion.101
  408.9 5.9 %fusion.66 = f32[2048,1024]{1,0:T(8,128)} fusion(bf16[128,2048]{1,0:T(8,128)(2,1)} %copy-done.7, f32[128,1024]{1,0:T(8,128)S(1)} %copy.91, bf16[128,1024]{1,0:T(8,128)(2,1)} %param.25), kind=kOutput, calls=%fused_computation.129 | convolution fusion | flops 537788416 | bytes 9699328 | tf_op jit(solution)/shard_map/dot_general | solution.py:231
  417.7 2.3 copy.104
  421.7 2.4 copy.105
  424.1 2.8 fusion.2
  431.9 3.3 fusion.12
  440.3 6.7 %fusion.38 = f32[16]{0:T(128)S(1)} fusion(f32[16]{0:T(128)} %copy-done.73, f32[16]{0:T(128)S(1)} %copy-done.69, f32[16]{0:T(128)} %copy-done.70, f32[16]{0:T(128)} %copy-done.75, f32[16]{0:T(128)} %get-tuple-element.215, f32[16]{0:T(128)} %get-tuple-element.278, f32[16]{0:T(128)} %get-tuple-element.277, f32[16]{0:T(128)} %get-tuple-element.276, ...), kind=kLoop, calls=%fused_computation.61 | loop fusion | flops 11534320 | bytes 14682076 | tf_op jit(solution)/shard_map/transpose(jvp())/while/body/eval_jaxpr/reduce_sum | solution.py:61
  448.9 2.2 fusion.33
  451.2 114.9 %reduce-scatter.5.cloned.1.call-done = f32[32,1024]{1,0:T(8,128)} async-done(((f32[2048,1024]{1,0:T(8,128)}), f32[32,1024]{1,0:T(8,128)}) %reduce-scatter.5.cloned.1.call-update) | async-done | bytes 131088 | tf_op jit(solution)/shard_map/reduce_scatter | solution.py:230
  (354 shorter events, 69.0 us)
Async XLA Ops:
  8.0 38.6 %copy-start = (bf16[1,2048,256]{2,1,0:T(8,128)(2,1)S(1)}, bf16[1,2048,256]{2,1,0:T(8,128)(2,1)}, u32[]{:S(2)}) copy-start(bf16[1,2048,256]{2,1,0:T(8,128)(2,1)} %param.17) | copy-start | bytes 3145732
  8.0 38.5 %all-gather.16.cloned.1.call-start = ((), (), s32[]{:S(2)}) async-start(), calls=%async_computation.5 | async-start | bytes 1966080 | tf_op jit(solution)/shard_map/all_gather | solution.py:138
  8.8 63.9 %all-gather.14.cloned.1.call-start = ((), (), s32[]{:S(2)}) async-start(), calls=%async_computation.4 | async-start | bytes 1966080 | tf_op jit(solution)/shard_map/all_gather | solution.py:137
  46.5 72.9 %reduce-scatter.3.cloned.1.call-start = ((), (), s32[]{:S(2)}) async-start(), calls=%async_computation.6 | async-start | bytes 3932160 | tf_op jit(solution)/shard_map/reduce_scatter | solution.py:163
  78.7 53.4 %copy-start.48 = (bf16[128,256]{1,0:T(8,128)(2,1)S(1)}, bf16[128,256]{1,0:T(8,128)(2,1)}, u32[]{:S(2)}) copy-start(bf16[128,256]{1,0:T(8,128)(2,1)} %param.23) | copy-start | bytes 196612
  78.7 53.5 %copy-start.65 = (f32[128,16]{0,1:T(8,128)S(1)}, f32[128,16]{0,1:T(8,128)}, u32[]{:S(2)}) copy-start(f32[128,16]{0,1:T(8,128)} %param.24) | copy-start | bytes 24580
  78.7 91.5 %all-gather.24.cloned.1.call-start = ((), (), s32[]{:S(2)}) async-start(), calls=%async_computation.11 | async-start | bytes 4259840 | tf_op jit(solution)/shard_map/all_gather | solution.py:205
  121.5 32.9 %all-to-all-start.1 = ((bf16[64,6,512]{2,1,0:T(8,128)(2,1)}), bf16[64,6,512]{2,1,0:T(8,128)(2,1)S(1)}, u32[]{:S(2)}, u32[]{:S(2)}) async-start(bf16[64,6,512]{2,1,0:T(8,128)(2,1)} %reshape_transpose_reshape.7), calls=%async_computation.2 | async-start | bytes 1048576 | tf_op jit(solution)/shard_map/all_to_all | solution.py:168
  132.0 57.5 %all-gather.26.cloned.1.call-start = ((), (), s32[]{:S(2)}) async-start(), calls=%async_computation.12 | async-start | bytes 1572864 | tf_op jit(solution)/shard_map/all_gather | solution.py:24
  132.4 43.2 %copy-start.27 = (f32[128,16]{1,0:T(8,128)}, f32[128,16]{1,0:T(8,128)S(1)}, u32[]{:S(2)}) copy-start(f32[128,16]{1,0:T(8,128)S(1)} %reduce_window_sum.43) | copy-start | bytes 24580
  132.5 41.8 %copy-start.41 = (f32[128,2,8]{0,2,1:T(8,128)}, f32[128,2,8]{0,2,1:T(8,128)S(1)}, u32[]{:S(2)}) copy-start(f32[128,2,8]{0,2,1:T(8,128)S(1)} %bitcast_exponential_fusion) | copy-start | bytes 24580
  175.5 48.9 %all-gather.28.cloned.1.call-start = ((), (), s32[]{:S(2)}) async-start(), calls=%async_computation.13 | async-start | bytes 2621440 | tf_op jit(solution)/shard_map/all_gather | solution.py:24
  177.9 49.8 %copy-start.57 = (f32[2,1,16]{2,1,0:T(1,128)}, f32[2,1,16]{2,1,0:T(1,128)S(1)}, u32[]{:S(2)}) copy-start(f32[2,1,16]{2,1,0:T(1,128)S(1)} %all-gather) | copy-start | bytes 388
  188.9 40.1 %copy-start.50 = (f32[4,1,16]{2,1,0:T(1,128)}, f32[4,1,16]{2,1,0:T(1,128)S(1)}, u32[]{:S(2)}) copy-start(f32[4,1,16]{2,1,0:T(1,128)S(1)} %all-gather.1) | copy-start | bytes 772
  189.5 38.2 %copy-start.70 = (f32[16]{0:T(128)}, f32[16]{0:T(128)S(1)}, u32[]{:S(2)}) copy-start(f32[16]{0:T(128)S(1)} %get-tuple-element.279) | copy-start | bytes 196
  191.8 90.9 %all-gather.30.cloned.1.call-start = ((), (), s32[]{:S(2)}) async-start(), calls=%async_computation.14 | async-start | bytes 4718592 | tf_op jit(solution)/shard_map/all_gather | solution.py:24
  227.7 76.8 %all-gather.18.cloned.1.call-start = ((), (), s32[]{:S(2)}) async-start(), calls=%async_computation.7 | async-start | bytes 1572864 | tf_op jit(solution)/shard_map/all_gather | solution.py:24
  228.5 56.9 %copy-start.84 = (f32[2,8]{1,0:T(2,128)}, f32[2,8]{1,0:T(2,128)S(1)}, u32[]{:S(2)}) copy-start(f32[2,8]{1,0:T(2,128)S(1)} %squeeze.234) | copy-start | bytes 196
  228.6 56.9 %copy-start.76 = (f32[2,8]{1,0:T(2,128)}, f32[2,8]{1,0:T(2,128)S(1)}, u32[]{:S(2)}) copy-start(f32[2,8]{1,0:T(2,128)S(1)} %squeeze.235) | copy-start | bytes 196
  228.7 56.8 %copy-start.85 = (f32[2,8]{1,0:T(2,128)}, f32[2,8]{1,0:T(2,128)S(1)}, u32[]{:S(2)}) copy-start(f32[2,8]{1,0:T(2,128)S(1)} %squeeze.230) | copy-start | bytes 196
  228.8 56.7 %copy-start.53 = (f32[2,8]{1,0:T(2,128)}, f32[2,8]{1,0:T(2,128)S(1)}, u32[]{:S(2)}) copy-start(f32[2,8]{1,0:T(2,128)S(1)} %squeeze.231) | copy-start | bytes 196
  228.9 56.6 %copy-start.55 = (f32[2,8]{1,0:T(2,128)}, f32[2,8]{1,0:T(2,128)S(1)}, u32[]{:S(2)}) copy-start(f32[2,8]{1,0:T(2,128)S(1)} %squeeze.232) | copy-start | bytes 196
  229.0 56.5 %copy-start.78 = (f32[2,8]{1,0:T(2,128)}, f32[2,8]{1,0:T(2,128)S(1)}, u32[]{:S(2)}) copy-start(f32[2,8]{1,0:T(2,128)S(1)} %squeeze.233) | copy-start | bytes 196
  290.3 51.3 %copy-start.60 = (f32[16]{0:T(128)S(1)}, f32[16]{0:T(128)}, u32[]{:S(2)}) copy-start(f32[16]{0:T(128)} %copy-done.59) | copy-start | bytes 196
  290.3 51.3 %copy-start.63 = (f32[16]{0:T(128)S(1)}, f32[16]{0:T(128)}, u32[]{:S(2)}) copy-start(f32[16]{0:T(128)} %copy-done.62) | copy-start | bytes 196
  290.3 51.3 %copy-start.71 = (f32[16]{0:T(128)S(1)}, f32[16]{0:T(128)}, u32[]{:S(2)}) copy-start(f32[16]{0:T(128)} %get-tuple-element.280) | copy-start | bytes 196
  290.3 51.3 %copy-start.74 = (f32[16]{0:T(128)S(1)}, f32[16]{0:T(128)}, u32[]{:S(2)}) copy-start(f32[16]{0:T(128)} %get-tuple-element.283) | copy-start | bytes 196
  291.5 50.1 %all-gather.20.cloned.1.call-start = ((), (), s32[]{:S(2)}) async-start(), calls=%async_computation.8 | async-start | bytes 2621440 | tf_op jit(solution)/shard_map/all_gather | solution.py:24
  307.0 92.8 %all-gather.22.cloned.1.call-start = ((), (), s32[]{:S(2)}) async-start(), calls=%async_computation.9 | async-start | bytes 4718592 | tf_op jit(solution)/shard_map/all_gather | solution.py:24
  344.8 221.2 %reduce-scatter.5.cloned.1.call-start = ((), (), s32[]{:S(2)}) async-start(), calls=%async_computation.10 | async-start | bytes 8519680 | tf_op jit(solution)/shard_map/reduce_scatter | solution.py:230
  345.0 57.6 %copy-start.29 = (bf16[128,2,128]{0,2,1:T(8,128)(2,1)}, bf16[128,2,128]{0,2,1:T(8,128)(2,1)S(1)}, u32[]{:S(2)}) copy-start(bf16[128,2,128]{0,2,1:T(8,128)(2,1)S(1)} %copy.98) | copy-start | bytes 196612
  440.3 125.8 %copy-start.1 = (bf16[1,2048,256]{2,1,0:T(8,128)(2,1)S(1)}, bf16[1,2048,256]{2,1,0:T(8,128)(2,1)}, u32[]{:S(2)}) copy-start(bf16[1,2048,256]{2,1,0:T(8,128)(2,1)} %param.17) | copy-start | bytes 3145732
  (91 other events, 551.0 us)
Sparse Core Ops, SparseCore 0:
  10.6 30.5 all-gather.15
  46.6 26.0 all-gather.13
  78.8 40.6 reduce-scatter.2
  227.8 54.8 all-gather.29
  344.9 54.7 all-gather.21
Sparse Core Ops, SparseCore 1:
  81.9 83.9 all-gather.23
  175.6 11.8 all-gather.25
  191.9 32.5 all-gather.27
  291.6 12.8 all-gather.17
  307.0 34.5 all-gather.19
  414.9 151.1 reduce-scatter.4
where the time goes:
time: 574 us; the launch traced here: 573 us
  waiting for transfers between devices  340 us (59%)
  blocking collectives  87.1 us (15%)
  local copies, waits for them, and re-layouts  40.5 us (7%)
  matrix products  39.5 us (7%)
  other arithmetic  38.5 us (7%)
  between operations  16.7 us (3%)
  starting transfers between devices  10.9 us (2%)
    all_gather x6, waiting for transfers between devices, carried_in(): pieces = jax.tree.map(lambda part: lax.all_gather(part, axis), running)  140 us
    reduce_scatter x1, waiting for transfers between devices, shards(): lax.psum_scatter(lax.dot_general(part_rows, mixed, (((0,), (0,)), ((), ()...  115 us
    all_gather x4, blocking collectives, carried_in(): pieces = jax.tree.map(lambda part: lax.all_gather(part, axis), running)  45.8 us
    reduce_scatter x1, waiting for transfers between devices, shards(): lax.psum_scatter(partial_value, 'tp', scatter_dimension=2, tiled=True)  40.2 us
    all_to_all x1, blocking collectives, shards(): lax.all_to_all(outgoing.reshape(experts_all, capacity, columns), SP, spli...  29.5 us
    all_gather x1, waiting for transfers between devices, shards(): arrived = lax.all_gather(arrived_part, 'tp', axis=2, tiled=True)  22 us
    all_to_all x1, waiting for transfers between devices, shards(): lax.all_to_all(send_back, SP, split_axis=0, concat_axis=0, tiled=True)  21.9 us
    add x6, other arithmetic, carry_combine(): later[0][:, None, None] * earlier[1] + later[1]  15.2 us
  transfers between devices with their start and end apart: 12, of which 9 were waited for; matrix products, arithmetic and copies ran while one was open for 13% of the time, Pallas kernels for 0%

commit v1 on v0

--- a/solution.py
+++ b/solution.py
@@ -134,7 +134,9 @@
         arrived_part.reshape(sp_size, local_experts, capacity, columns), 0, 1
     )
     arrived_part = arrived_part.reshape(local_experts, slot_count, columns)
-    arrived = lax.all_gather(arrived_part, "tp", axis=2, tiled=True)
+    arrived = jnp.concatenate(
+        lax.all_to_all(jnp.stack([arrived_part] * lax.axis_size("tp")), "tp", 0, 0), axis=2
+    )
     full_rows = lax.all_gather(expert_rows, "tp", axis=2, tiled=True)
     gate_pre = jnp.einsum("esd,edf->esf", full_rows, w_gate, preferred_element_type=jnp.float32)
     up_pre = jnp.einsum("esd,edf->esf", full_rows, w_up, preferred_element_type=jnp.float32)

time: 574 us -> 568 us (0.990)
  waiting for transfers between devices: 340 us -> 328 us
    all_gather x1 -> x0, waiting for transfers between devices: 22 us -> none  [shards(): arrived = lax.all_gather(arrived_part, 'tp', axis=2, tiled=True)]
    all_to_all x0 -> x1, waiting for transfers between devices: none -> 14.3 us  [shards(): lax.all_to_all(jnp.stack([arrived_part] * lax.axis_size('tp')), 'tp', 0, 0)]
where the time goes in v1:
time: 568 us; the launch traced here: 567 us
  waiting for transfers between devices  328 us (58%)
  blocking collectives  87.2 us (15%)
  local copies, waits for them, and re-layouts  41.2 us (7%)
  matrix products  39.9 us (7%)
  other arithmetic  38.6 us (7%)
  between operations  16.7 us (3%)
  starting transfers between devices  15.7 us (3%)
    all_gather x6, waiting for transfers between devices, carried_in(): pieces = jax.tree.map(lambda part: lax.all_gather(part, axis), running)  140 us
    reduce_scatter x1, waiting for transfers between devices, shards(): lax.psum_scatter(lax.dot_general(part_rows, mixed, (((0,), (0,)), ((), ()...  115 us
    all_gather x4, blocking collectives, carried_in(): pieces = jax.tree.map(lambda part: lax.all_gather(part, axis), running)  45.7 us
    reduce_scatter x1, waiting for transfers between devices, shards(): lax.psum_scatter(partial_value, 'tp', scatter_dimension=2, tiled=True)  35.6 us
    all_to_all x1, blocking collectives, shards(): lax.all_to_all(outgoing.reshape(experts_all, capacity, columns), SP, spli...  29.5 us
    all_to_all x1, waiting for transfers between devices, shards(): lax.all_to_all(send_back, SP, split_axis=0, concat_axis=0, tiled=True)  21.9 us
    add x6, other arithmetic, carry_combine(): later[0][:, None, None] * earlier[1] + later[1]  15.2 us
    all_to_all x1, waiting for transfers between devices, shards(): lax.all_to_all(jnp.stack([arrived_part] * lax.axis_size('tp')), 'tp', 0, 0)  14.3 us
  transfers between devices with their start and end apart: 12, of which 9 were waited for; matrix products, arithmetic and copies ran while one was open for 13% of the time, Pallas kernels for 0%

profile of v1, /device:TPU:4, one launch (start us, length us, event | category | flops | bytes accessed | tf_op | source)
XLA Modules:
  0.0 566.9 jit_solution(13643703318824444102)
XLA Ops:
  16.0 29.5 %all_to_all.15 = bf16[64,6,512]{2,1,0:T(8,128)(2,1)S(1)} all-to-all(bf16[64,6,512]{2,1,0:T(8,128)(2,1)S(1)} %reshape.701), channel_id=1, replica_groups=mesh['sp_0'=8,'sp_1'=4,'sp_2'=2,'tp'=4] {'sp_0','sp_1','sp_2'}, dimensions={0} | all-to-all | bytes 786432 | tf_op jit(solution)/shard_map/all_to_all | solution.py:126
  47.2 4.8 all-to-all-start.1
  56.1 14.3 %all-to-all-done.1 = bf16[4,1,384,512]{2,3,1,0:T(8,128)(2,1)} async-done(((bf16[4,1,384,512]{2,3,1,0:T(8,128)(2,1)}), bf16[4,1,384,512]{2,3,1,0:T(8,128)(2,1)}, u32[]{:S(2)}, u32[]{:S(2)}) %all-to-all-start.1) | async-done | bytes 1572896 | tf_op jit(solution)/shard_map/all_to_all | solution.py:138
  70.4 2.3 multiply_convert_fusion.3
  77.0 35.6 %reduce-scatter.3.cloned.1.call-done = f32[1,384,512]{2,1,0:T(8,128)} async-done(((f32[1,384,2048]{2,1,0:T(8,128)}), f32[1,384,512]{2,1,0:T(8,128)}) %reduce-scatter.3.cloned.1.call-update) | async-done | bytes 786448 | tf_op jit(solution)/shard_map/reduce_scatter | solution.py:165
  114.8 10.5 %all-to-all-start.2 = ((bf16[64,6,512]{2,1,0:T(8,128)(2,1)}), bf16[64,6,512]{2,1,0:T(8,128)(2,1)S(1)}, u32[]{:S(2)}, u32[]{:S(2)}) async-start(bf16[64,6,512]{2,1,0:T(8,128)(2,1)} %reshape_transpose_reshape.3), calls=%async_computation.3 | async-start | bytes 1048576 | tf_op jit(solution)/shard_map/all_to_all | solution.py:170
  125.7 21.9 %all-to-all-done.2 = bf16[64,6,512]{2,1,0:T(8,128)(2,1)S(1)} async-done(((bf16[64,6,512]{2,1,0:T(8,128)(2,1)}), bf16[64,6,512]{2,1,0:T(8,128)(2,1)S(1)}, u32[]{:S(2)}, u32[]{:S(2)}) %all-to-all-start.2) | async-done | bytes 393248 | tf_op jit(solution)/shard_map/all_to_all | solution.py:170
  151.6 12.0 %all_gather.52 = bf16[128,2048]{1,0:T(8,128)(2,1)S(1)} all-gather(bf16[128,512]{1,0:T(8,128)(2,1)S(1)} %get-tuple-element.222), channel_id=1, replica_groups=mesh['sp_0'=8,'sp_1'=4,'sp_2'=2,'tp'=4] {'tp'}, dimensions={1}, use_global_device_ids=true | all-gather | bytes 655360 | tf_op jit(solution)/shard_map/all_gather | solution.py:178
  163.6 4.0 fusion.70
  171.9 10.3 %all-gather.1 = f32[4,1,16]{2,1,0:T(1,128)S(1)} all-gather(f32[1,1,16]{2,1,0:T(1,128)S(1)} %get-tuple-element.301), channel_id=1, replica_groups=mesh['sp_0'=8,'sp_1'=4,'sp_2'=2,'tp'=4] {'sp_1'}, dimensions={0}, use_global_device_ids=true | all-gather | bytes 320 | tf_op jit(solution)/shard_map/all_gather | solution.py:24
  182.9 2.3 multiply_add_fusion.1
  185.8 32.2 %all-gather.25.cloned.1.call-done = f32[4,16,64,128]{3,2,1,0:T(8,128)} async-done(((f32[1,16,64,128]{3,2,1,0:T(8,128)}), f32[4,16,64,128]{3,2,1,0:T(8,128)}) %all-gather.25.cloned.1.call-update) | async-done | bytes 2097168 | tf_op jit(solution)/shard_map/all_gather | solution.py:24
  218.0 3.3 multiply_add_fusion
  223.2 16.8 %all-gather.3 = f32[8,1,16]{2,1,0:T(1,128)S(1)} all-gather(f32[1,1,16]{2,1,0:T(1,128)S(1)} %get-tuple-element.282), channel_id=1, replica_groups=mesh['sp_0'=8,'sp_1'=4,'sp_2'=2,'tp'=4] {'sp_0'}, dimensions={0}, use_global_device_ids=true | all-gather | bytes 576 | tf_op jit(solution)/shard_map/all_gather | solution.py:24
  246.6 29.7 %all-gather.27.cloned.1.call-done = f32[8,16,64,128]{3,2,1,0:T(8,128)} async-done(((f32[1,16,64,128]{3,2,1,0:T(8,128)}), f32[8,16,64,128]{3,2,1,0:T(8,128)}) %all-gather.27.cloned.1.call-update) | async-done | bytes 4194320 | tf_op jit(solution)/shard_map/all_gather | solution.py:24
  276.4 2.6 fusion.100
  279.3 2.6 add_add_fusion
  285.1 12.9 %all-gather.15.cloned.1.call-done = f32[2,16,64,128]{3,2,1,0:T(8,128)} async-done(((f32[1,16,64,128]{3,2,1,0:T(8,128)}), f32[2,16,64,128]{3,2,1,0:T(8,128)}) %all-gather.15.cloned.1.call-update) | async-done | bytes 1048592 | tf_op jit(solution)/shard_map/all_gather | solution.py:24
  298.0 2.4 multiply_add_fusion.3
  300.6 34.7 %all-gather.17.cloned.1.call-done = f32[4,16,64,128]{3,2,1,0:T(8,128)} async-done(((f32[1,16,64,128]{3,2,1,0:T(8,128)}), f32[4,16,64,128]{3,2,1,0:T(8,128)}) %all-gather.17.cloned.1.call-update) | async-done | bytes 2097168 | tf_op jit(solution)/shard_map/all_gather | solution.py:24
  335.3 3.2 multiply_add_fusion.2
  338.9 16.7 %all-gather.2 = f32[8,1,16]{2,1,0:T(1,128)S(1)} all-gather(f32[1,1,16]{2,1,0:T(1,128)S(1)} %copy-done.87), channel_id=1, replica_groups=mesh['sp_0'=8,'sp_1'=4,'sp_2'=2,'tp'=4] {'sp_0'}, dimensions={0}, use_global_device_ids=true | all-gather | bytes 576 | tf_op jit(solution)/shard_map/all_gather | solution.py:24
  363.1 30.4 %all-gather.19.cloned.1.call-done = f32[8,16,64,128]{3,2,1,0:T(8,128)} async-done(((f32[1,16,64,128]{3,2,1,0:T(8,128)}), f32[8,16,64,128]{3,2,1,0:T(8,128)}) %all-gather.19.cloned.1.call-update) | async-done | bytes 4194320 | tf_op jit(solution)/shard_map/all_gather | solution.py:24
  393.6 2.6 fusion.99
  402.5 5.9 %fusion.64 = f32[2048,1024]{1,0:T(8,128)} fusion(bf16[128,2048]{1,0:T(8,128)(2,1)} %copy-done.7, f32[128,1024]{1,0:T(8,128)S(1)} %copy.94, bf16[128,1024]{1,0:T(8,128)(2,1)} %param.25), kind=kOutput, calls=%fused_computation.127 | convolution fusion | flops 537788416 | bytes 9699328 | tf_op jit(solution)/shard_map/dot_general | solution.py:233
  411.4 2.3 copy.107
  415.4 2.3 copy.108
  417.7 3.2 fusion.2
  425.9 3.3 fusion.9
  434.3 6.7 %fusion.36 = f32[16]{0:T(128)S(1)} fusion(f32[16]{0:T(128)} %copy-done.69, f32[16]{0:T(128)S(1)} %copy-done.65, f32[16]{0:T(128)} %copy-done.66, f32[16]{0:T(128)} %copy-done.71, f32[16]{0:T(128)} %get-tuple-element.215, f32[16]{0:T(128)} %get-tuple-element.278, f32[16]{0:T(128)} %get-tuple-element.277, f32[16]{0:T(128)} %get-tuple-element.276, ...), kind=kLoop, calls=%fused_computation.59 | loop fusion | flops 11534320 | bytes 14682076 | tf_op jit(solution)/shard_map/transpose(jvp())/while/body/eval_jaxpr/reduce_sum | solution.py:61
  443.0 2.2 fusion.31
  445.2 114.5 %reduce-scatter.5.cloned.1.call-done = f32[32,1024]{1,0:T(8,128)} async-done(((f32[2048,1024]{1,0:T(8,128)}), f32[32,1024]{1,0:T(8,128)}) %reduce-scatter.5.cloned.1.call-update) | async-done | bytes 131088 | tf_op jit(solution)/shard_map/reduce_scatter | solution.py:232
  (355 shorter events, 71.9 us)
Async XLA Ops:
  8.0 44.0 %copy-start = (bf16[1,2048,256]{2,1,0:T(8,128)(2,1)S(1)}, bf16[1,2048,256]{2,1,0:T(8,128)(2,1)}, u32[]{:S(2)}) copy-start(bf16[1,2048,256]{2,1,0:T(8,128)(2,1)} %param.17) | copy-start | bytes 3145732
  8.0 44.0 %all-gather.13.cloned.1.call-start = ((), (), s32[]{:S(2)}) async-start(), calls=%async_computation.5 | async-start | bytes 1966080 | tf_op jit(solution)/shard_map/all_gather | solution.py:140
  47.2 23.2 %all-to-all-start.1 = ((bf16[4,1,384,512]{2,3,1,0:T(8,128)(2,1)}), bf16[4,1,384,512]{2,3,1,0:T(8,128)(2,1)}, u32[]{:S(2)}, u32[]{:S(2)}) async-start(bf16[4,1,384,512]{2,3,1,0:T(8,128)(2,1)} %stack.3), calls=%async_computation.1 | async-start | bytes 3145728 | tf_op jit(solution)/shard_map/all_to_all | solution.py:138
  52.0 60.7 %reduce-scatter.3.cloned.1.call-start = ((), (), s32[]{:S(2)}) async-start(), calls=%async_computation.6 | async-start | bytes 3932160 | tf_op jit(solution)/shard_map/reduce_scatter | solution.py:165
  76.4 48.9 %copy-start.44 = (bf16[128,256]{1,0:T(8,128)(2,1)S(1)}, bf16[128,256]{1,0:T(8,128)(2,1)}, u32[]{:S(2)}) copy-start(bf16[128,256]{1,0:T(8,128)(2,1)} %param.23) | copy-start | bytes 196612
  76.4 48.9 %copy-start.61 = (f32[128,16]{0,1:T(8,128)S(1)}, f32[128,16]{0,1:T(8,128)}, u32[]{:S(2)}) copy-start(f32[128,16]{0,1:T(8,128)} %param.24) | copy-start | bytes 24580
  76.5 87.1 %all-gather.21.cloned.1.call-start = ((), (), s32[]{:S(2)}) async-start(), calls=%async_computation.11 | async-start | bytes 4259840 | tf_op jit(solution)/shard_map/all_gather | solution.py:207
  114.8 32.9 %all-to-all-start.2 = ((bf16[64,6,512]{2,1,0:T(8,128)(2,1)}), bf16[64,6,512]{2,1,0:T(8,128)(2,1)S(1)}, u32[]{:S(2)}, u32[]{:S(2)}) async-start(bf16[64,6,512]{2,1,0:T(8,128)(2,1)} %reshape_transpose_reshape.3), calls=%async_computation.3 | async-start | bytes 1048576 | tf_op jit(solution)/shard_map/all_to_all | solution.py:170
  125.3 57.6 %all-gather.23.cloned.1.call-start = ((), (), s32[]{:S(2)}) async-start(), calls=%async_computation.12 | async-start | bytes 1572864 | tf_op jit(solution)/shard_map/all_gather | solution.py:24
  125.6 43.4 %copy-start.26 = (f32[128,16]{1,0:T(8,128)}, f32[128,16]{1,0:T(8,128)S(1)}, u32[]{:S(2)}) copy-start(f32[128,16]{1,0:T(8,128)S(1)} %reduce_window_sum.43) | copy-start | bytes 24580
  125.7 42.0 %copy-start.37 = (f32[128,2,8]{0,2,1:T(8,128)}, f32[128,2,8]{0,2,1:T(8,128)S(1)}, u32[]{:S(2)}) copy-start(f32[128,2,8]{0,2,1:T(8,128)S(1)} %bitcast_exponential_fusion) | copy-start | bytes 24580
  168.9 49.1 %all-gather.25.cloned.1.call-start = ((), (), s32[]{:S(2)}) async-start(), calls=%async_computation.13 | async-start | bytes 2621440 | tf_op jit(solution)/shard_map/all_gather | solution.py:24
  171.3 49.9 %copy-start.53 = (f32[2,1,16]{2,1,0:T(1,128)}, f32[2,1,16]{2,1,0:T(1,128)S(1)}, u32[]{:S(2)}) copy-start(f32[2,1,16]{2,1,0:T(1,128)S(1)} %all-gather) | copy-start | bytes 388
  182.2 40.4 %copy-start.46 = (f32[4,1,16]{2,1,0:T(1,128)}, f32[4,1,16]{2,1,0:T(1,128)S(1)}, u32[]{:S(2)}) copy-start(f32[4,1,16]{2,1,0:T(1,128)S(1)} %all-gather.1) | copy-start | bytes 772
  182.8 38.4 %copy-start.66 = (f32[16]{0:T(128)}, f32[16]{0:T(128)S(1)}, u32[]{:S(2)}) copy-start(f32[16]{0:T(128)S(1)} %get-tuple-element.279) | copy-start | bytes 196
  185.2 91.1 %all-gather.27.cloned.1.call-start = ((), (), s32[]{:S(2)}) async-start(), calls=%async_computation.14 | async-start | bytes 4718592 | tf_op jit(solution)/shard_map/all_gather | solution.py:24
  221.3 76.7 %all-gather.15.cloned.1.call-start = ((), (), s32[]{:S(2)}) async-start(), calls=%async_computation.7 | async-start | bytes 1572864 | tf_op jit(solution)/shard_map/all_gather | solution.py:24
  222.2 56.8 %copy-start.80 = (f32[2,8]{1,0:T(2,128)}, f32[2,8]{1,0:T(2,128)S(1)}, u32[]{:S(2)}) copy-start(f32[2,8]{1,0:T(2,128)S(1)} %squeeze.234) | copy-start | bytes 196
  222.3 56.7 %copy-start.72 = (f32[2,8]{1,0:T(2,128)}, f32[2,8]{1,0:T(2,128)S(1)}, u32[]{:S(2)}) copy-start(f32[2,8]{1,0:T(2,128)S(1)} %squeeze.235) | copy-start | bytes 196
  222.4 56.7 %copy-start.81 = (f32[2,8]{1,0:T(2,128)}, f32[2,8]{1,0:T(2,128)S(1)}, u32[]{:S(2)}) copy-start(f32[2,8]{1,0:T(2,128)S(1)} %squeeze.230) | copy-start | bytes 196
  222.4 56.6 %copy-start.49 = (f32[2,8]{1,0:T(2,128)}, f32[2,8]{1,0:T(2,128)S(1)}, u32[]{:S(2)}) copy-start(f32[2,8]{1,0:T(2,128)S(1)} %squeeze.231) | copy-start | bytes 196
  222.5 56.5 %copy-start.51 = (f32[2,8]{1,0:T(2,128)}, f32[2,8]{1,0:T(2,128)S(1)}, u32[]{:S(2)}) copy-start(f32[2,8]{1,0:T(2,128)S(1)} %squeeze.232) | copy-start | bytes 196
  222.6 56.4 %copy-start.74 = (f32[2,8]{1,0:T(2,128)}, f32[2,8]{1,0:T(2,128)S(1)}, u32[]{:S(2)}) copy-start(f32[2,8]{1,0:T(2,128)S(1)} %squeeze.233) | copy-start | bytes 196
  283.8 51.5 %copy-start.56 = (f32[16]{0:T(128)S(1)}, f32[16]{0:T(128)}, u32[]{:S(2)}) copy-start(f32[16]{0:T(128)} %copy-done.55) | copy-start | bytes 196
  283.8 51.5 %copy-start.59 = (f32[16]{0:T(128)S(1)}, f32[16]{0:T(128)}, u32[]{:S(2)}) copy-start(f32[16]{0:T(128)} %copy-done.58) | copy-start | bytes 196
  283.8 51.5 %copy-start.67 = (f32[16]{0:T(128)S(1)}, f32[16]{0:T(128)}, u32[]{:S(2)}) copy-start(f32[16]{0:T(128)} %get-tuple-element.280) | copy-start | bytes 196
  283.8 51.5 %copy-start.70 = (f32[16]{0:T(128)S(1)}, f32[16]{0:T(128)}, u32[]{:S(2)}) copy-start(f32[16]{0:T(128)} %get-tuple-element.283) | copy-start | bytes 196
  285.1 50.2 %all-gather.17.cloned.1.call-start = ((), (), s32[]{:S(2)}) async-start(), calls=%async_computation.8 | async-start | bytes 2621440 | tf_op jit(solution)/shard_map/all_gather | solution.py:24
  300.5 92.9 %all-gather.19.cloned.1.call-start = ((), (), s32[]{:S(2)}) async-start(), calls=%async_computation.9 | async-start | bytes 4718592 | tf_op jit(solution)/shard_map/all_gather | solution.py:24
  338.6 221.2 %reduce-scatter.5.cloned.1.call-start = ((), (), s32[]{:S(2)}) async-start(), calls=%async_computation.10 | async-start | bytes 8519680 | tf_op jit(solution)/shard_map/reduce_scatter | solution.py:232
  338.8 57.5 %copy-start.28 = (bf16[128,2,128]{0,2,1:T(8,128)(2,1)}, bf16[128,2,128]{0,2,1:T(8,128)(2,1)S(1)}, u32[]{:S(2)}) copy-start(bf16[128,2,128]{0,2,1:T(8,128)(2,1)S(1)} %copy.101) | copy-start | bytes 196612
  434.3 125.4 %copy-start.1 = (bf16[1,2048,256]{2,1,0:T(8,128)(2,1)S(1)}, bf16[1,2048,256]{2,1,0:T(8,128)(2,1)}, u32[]{:S(2)}) copy-start(bf16[1,2048,256]{2,1,0:T(8,128)(2,1)} %param.17) | copy-start | bytes 3145732
  (91 other events, 537.1 us)
Sparse Core Ops, SparseCore 0:
  10.6 30.5 all-gather.12
  76.5 36.0 reduce-scatter.2
  185.3 32.6 all-gather.24
  300.6 34.6 all-gather.16
Sparse Core Ops, SparseCore 1:
  79.7 79.4 all-gather.20
  169.0 11.8 all-gather.22
  221.4 54.8 all-gather.26
  285.1 12.8 all-gather.14
  338.6 54.7 all-gather.18
  408.5 151.1 reduce-scatter.4
